TPU v7x, 32 devices: a whole 2x2x4 slice. The times are simulated.
32 devices in a mesh: sp: 16 (over z, y, x), tp: 2 (over core).
Axes of the slice: x: 2, y: 2, z: 4, core: 2. Of those that a mesh axis runs over, the one named last changes fastest.
Arguments:
- queries: bfloat16 [8192, 1024], P('sp', 'tp'), may hold values from -8 to 8
- key_rows: bfloat16 [8192, 512], P('sp', 'tp'), may hold values from -8 to 8
- values: bfloat16 [8192, 512], P('sp', 'tp'), may hold values from -16 to 16
- doc_ids: int32 [8192], P('sp'), may hold values from 0 to 7, never falling along the last dimension, each value on 1 to 2048 neighbouring positions
- sink_logits: float32 [16], P('tp'), may hold values from 2.5 to 6
- residual: bfloat16 [8192, 2048], P('sp'), may hold values from -6 to 6
- out_weight: bfloat16 [1024, 2048], P('tp'), may hold values from -0.1875 to 0.1875
- norm_gain: float32 [2048], replicated, may hold values from 0.1 to 1.9
- w_gate: bfloat16 [2048, 5632], P('sp', 'tp'), may hold values from -0.125 to 0.125
- w_up: bfloat16 [2048, 5632], P('sp', 'tp'), may hold values from -0.125 to 0.125
- w_down: bfloat16 [5632, 2048], P('tp', 'sp'), may hold values from -0.078125 to 0.078125
Outputs:
- layer_out: bfloat16 [8192, 2048], P('sp')
Inputs may be any that keep to these rules, and one draw needn't show every extreme that they name: `doc_ids`: document numbers never fall along the positions; each document has 1 to 2048 positions.
All inputs are finite; a program needn't handle non-finite values.
Results may differ from a plain program's by a relative error of at most 0.014.
Values may be sent and summed in bfloat16 or wider, within the bound.
A program may use at most 128 MiB of HBM per device.

v0:
```python
import jax
import jax.numpy as jnp
from jax import lax
from jax.experimental import pallas as pl
from jax.experimental.pallas import tpu as pltpu
from jax.sharding import PartitionSpec as P


HD = 64
WINDOW = 128
INNER = 4
CHUNKS = 2


def from_behind(shard, axis, by):
    size = lax.axis_size(axis)
    pairs = [(i, i + by) for i in range(size) if 0 <= i + by < size]
    return lax.ppermute(shard, axis, pairs)


def rms_norm(stream, norm_gain):
    floats = stream.astype(jnp.float32)
    scale = lax.rsqrt(jnp.mean(floats * floats, axis=-1, keepdims=True) + 1e-06)
    return floats * scale * norm_gain


def band_rows(tensor, blocks):
    tensor = tensor.reshape((blocks + 1, WINDOW) + tensor.shape[1:])
    return jnp.concatenate([tensor[:-1], tensor[1:]], axis=1)


def attend(queries, key_rows, values, doc_ids, sink_logits):
    local_rows = queries.shape[0]
    blocks = local_rows // WINDOW
    kv_local = key_rows.shape[1] // HD
    per_kv = queries.shape[1] // key_rows.shape[1]
    tail_docs = doc_ids[local_rows - WINDOW :] + 1
    width = key_rows.shape[1]
    tail = jnp.concatenate(
        [
            key_rows[local_rows - WINDOW :],
            values[local_rows - WINDOW :],
            jnp.broadcast_to(tail_docs.astype(jnp.bfloat16)[:, None], (WINDOW, 128)),
        ],
        axis=1,
    )
    tail = from_behind(tail, "sp", 1)
    prev_keys, prev_values = tail[:, :width], tail[:, width : 2 * width]
    prev_docs = tail[:, 2 * width].astype(jnp.int32)
    key_band = band_rows(jnp.concatenate([prev_keys, key_rows], axis=0), blocks).reshape(
        blocks, 2 * WINDOW, kv_local, HD
    )
    value_band = band_rows(jnp.concatenate([prev_values, values], axis=0), blocks).reshape(
        blocks, 2 * WINDOW, kv_local, HD
    )
    doc_band = band_rows(jnp.concatenate([prev_docs - 1, doc_ids]), blocks)
    query_band = queries.reshape(blocks, WINDOW, kv_local, per_kv, HD)
    scores = jnp.einsum(
        "nqhgd,nkhd->nhgqk", query_band, key_band, preferred_element_type=jnp.float32
    ) * HD ** (-0.5)
    offsets = jnp.arange(WINDOW)[:, None] + WINDOW - jnp.arange(2 * WINDOW)[None, :]
    inside = (offsets >= 0) & (offsets < WINDOW)
    query_docs = doc_ids.reshape(blocks, WINDOW)
    allowed = inside[None] & (query_docs[:, :, None] == doc_band[:, None, :])
    scores = jnp.where(allowed[:, None, None], scores, -1e30)
    sink_logit = sink_logits.reshape(kv_local, per_kv)[None, :, :, None, None]
    peak = jnp.maximum(jnp.max(scores, axis=-1, keepdims=True), sink_logit)
    raised = jnp.exp(scores - peak)
    denom = jnp.sum(raised, axis=-1, keepdims=True) + jnp.exp(sink_logit - peak)
    weights = (raised / denom).astype(jnp.bfloat16)
    attended = jnp.einsum(
        "nhgqk,nkhd->nqhgd", weights, value_band, preferred_element_type=jnp.float32
    )
    return attended.astype(jnp.bfloat16).reshape(local_rows, queries.shape[1])


def swap(shard, axis, by):
    size = lax.axis_size(axis)
    return lax.ppermute(shard, axis, [(i, i ^ by) for i in range(size)])


def piece_of(tensor, index, axis, pieces):
    size = tensor.shape[axis] // pieces
    return lax.dynamic_slice_in_dim(tensor, index * size, size, axis)


def in_order(mine, others, place, axis):
    size = mine.shape[axis]
    shape = list(mine.shape)
    shape[axis] = size * (len(others) + 1)
    whole = jnp.zeros(shape, mine.dtype)
    for k, shard in enumerate([mine] + others):
        whole = lax.dynamic_update_slice_in_dim(whole, shard, (place ^ k) * size, axis)
    return whole


def on_device(
    queries,
    key_rows,
    values,
    doc_ids,
    sink_logits,
    residual,
    out_weight,
    norm_gain,
    w_gate,
    w_up,
    w_down,
):
    inner = INNER
    outer = lax.axis_size("sp") // inner
    tp = lax.axis_size("tp")
    seat = lax.rem(lax.axis_index("sp"), inner)
    core = lax.axis_index("tp")
    columns = [[row + inner * step for step in range(outer)] for row in range(inner)]

    def gate_up_piece(k):
        return jnp.concatenate(
            [piece_of(w_gate, seat ^ k, 1, inner), piece_of(w_up, seat ^ k, 1, inner)], axis=1
        )

    def down_piece(k):
        return piece_of(w_down, seat ^ k, 0, inner)[None]

    gate_up_pieces = [gate_up_piece(k) for k in range(inner)]
    gate_up_pieces, queries, key_rows, values, w_down = lax.optimization_barrier(
        (gate_up_pieces, queries, key_rows, values, w_down)
    )
    gate_up = in_order(
        gate_up_pieces[0], [swap(gate_up_pieces[k], "sp", k) for k in range(1, inner)], seat, 0
    )
    down = in_order(
        down_piece(0), [swap(down_piece(k), "sp", k) for k in range(1, inner)], seat, 0
    )

    def across(block):
        return lax.all_gather(block, "sp", axis=0, tiled=True, axis_index_groups=columns)

    def flat(gathered):
        return jnp.swapaxes(gathered, 0, 1).reshape(gathered.shape[1], -1)

    part = inner // CHUNKS
    gate_up = across(gate_up)
    downs = []
    for c in range(CHUNKS):
        downs.append(across(down[c * part : (c + 1) * part]))

    attended = attend(queries, key_rows, values, doc_ids, sink_logits)
    mix_term = jnp.dot(attended, out_weight, preferred_element_type=jnp.float32).astype(jnp.bfloat16)
    mixed_sum = piece_of(mix_term, core, 0, tp).astype(jnp.float32)
    for k in range(1, tp):
        mixed_sum += swap(piece_of(mix_term, core ^ k, 0, tp), "tp", k).astype(jnp.float32)
    stream = (piece_of(residual, core, 0, tp).astype(jnp.float32) + mixed_sum).astype(jnp.bfloat16)
    normed = rms_norm(stream, norm_gain).astype(jnp.bfloat16)
    rows, width = normed.shape
    near = jnp.concatenate([normed] + [swap(normed, "sp", k) for k in range(1, inner)], axis=0)
    tokens = jnp.concatenate([near] + [swap(near, "tp", k) for k in range(1, tp)], axis=0)

    acts = jnp.dot(tokens, gate_up, preferred_element_type=jnp.float32)
    units = acts.shape[1] // 2
    hidden = (jax.nn.silu(acts[:, :units]) * acts[:, units:]).astype(jnp.bfloat16)
    block = width // (outer * CHUNKS)
    outs = []
    for c in range(CHUNKS):
        mlp_term = jnp.dot(hidden, lax.optimization_barrier(flat(downs[c])), preferred_element_type=jnp.float32)
        mlp_term = mlp_term.astype(jnp.bfloat16).reshape(tp, inner * rows, width // CHUNKS)
        near_sum = mlp_term[0].astype(jnp.float32)
        for k in range(1, tp):
            near_sum += swap(mlp_term[k], "tp", k).astype(jnp.float32)
        near_sum = near_sum.reshape(inner, rows, width // CHUNKS)
        sends = [near_sum[k].astype(jnp.bfloat16) for k in range(1, inner)]
        total = near_sum[0]
        for k in range(1, inner):
            sent = swap(sends[k - 1], "sp", k)
            total += sent.astype(jnp.float32)
        outs.append(total)
    total = jnp.concatenate(
        [outs[c][:, o * block : (o + 1) * block] for o in range(outer) for c in range(CHUNKS)],
        axis=1,
    )
    out = (stream.astype(jnp.float32) + total).astype(jnp.bfloat16)
    return in_order(out, [swap(out, "tp", k) for k in range(1, tp)], core, 0)


def staged_solution(mesh):
    in_specs = (
        P("sp", "tp"),
        P("sp", "tp"),
        P("sp", "tp"),
        P("sp"),
        P("tp"),
        P("sp", None),
        P("tp", None),
        P(),
        P("sp", "tp"),
        P("sp", "tp"),
        P("tp", "sp"),
    )
    out_specs = P("sp", None)

    return jax.shard_map(
        on_device, mesh=mesh, in_specs=in_specs, out_specs=out_specs, check_vma=False
    )


MESH = pl.DeviceIdType.MESH
GATE_UP, DOWN = 0, 1


def layer_kernel(
    q_hbm, k_hbm, v_hbm, docs_hbm, sink_ref, res_hbm, ow_hbm, gain_ref, gate_hbm, up_hbm, down_hbm,
    o_hbm,
    wgu, wd, xbuf, acts, hid, pbuf, zbuf, rx, rz, own, qbuf, kbuf, vbuf, dbuf, att, ow,
    mix_out, mix_own, mix_in, res, obuf,
    load_sem, halo_s, halo_r, first_s, local_sem, far_s, y_s, sib_s, piece_r, sib_r,
    mix_s, mix_r, tok_s, tok_r, rx_s, rx_r, rz_s, rz_r, out_l, out_s, out_r,
):
    sp, c = lax.axis_index("sp"), lax.axis_index("tp")
    n_sp = lax.axis_size("sp")
    x, y, z = lax.rem(sp, 2), lax.rem(lax.div(sp, 2), 2), lax.div(sp, 4)
    l, h = lax.rem(z, 2), lax.div(z, 2)
    far, near = 2 * (1 - h) + l, 2 * h + 1 - l
    inner, outer = z * (3 - z) == 2, z * (3 - z) == 0
    planes = (z, z + 1 - 2 * h, far, 3 * (1 - l))
    depth, units = gate_hbm.shape[0], gate_hbm.shape[1] // 2
    half_units = units // 2
    rows, width = res_hbm.shape
    half = rows // 2
    blocks = rows // WINDOW
    kv_local = k_hbm.shape[1] // HD
    per_kv = q_hbm.shape[1] // k_hbm.shape[1]
    slab = 4 * depth

    def at(x_, y_, z_, c_):
        return {"sp": 4 * z_ + 2 * y_ + x_, "tp": c_}

    sibling = at(x, y, z, 1 - c)
    x_peer, z_peer = at(1 - x, y, z, c), at(x, y, near, c)

    def remote(src, dst, ss, rs, dev):
        return pltpu.make_async_remote_copy(
            src_ref=src, dst_ref=dst, send_sem=ss, recv_sem=rs, device_id=dev, device_id_type=MESH
        )

    def region(what, k, p):
        if what == GATE_UP:
            return wgu.at[
                pl.ds(pl.multiple_of(p * depth, depth), depth),
                pl.ds(pl.multiple_of(k * units, 128), units),
            ]
        return wd.at[
            pl.ds(pl.multiple_of(k * half_units, 16), half_units),
            pl.ds(pl.multiple_of(p * depth, depth), depth),
        ]

    def source(what, k, xq):
        if what == GATE_UP:
            return (gate_hbm, up_hbm)[k].at[:, pl.ds(pl.multiple_of(xq * units, 128), units)]
        return down_hbm.at[pl.ds(pl.multiple_of(xq * units + k * half_units, 16), half_units), :]

    def first_sends(what, act):
        for k in range(2):
            def copy_to(xq, z_, slot):
                return remote(
                    source(what, k, xq), region(what, k, sp), first_s.at[what, k, slot],
                    piece_r.at[what, sp], at(xq, y, z_, k),
                )

            @pl.when(l == c)
            def _():
                @pl.when(c == k)
                def _():
                    if act == "start":
                        pltpu.make_async_copy(
                            source(what, k, x), region(what, k, sp), local_sem.at[what]
                        ).start()

                @pl.when(c != k)
                def _():
                    getattr(copy_to(x, z, 0), act)()

                getattr(copy_to(1 - x, z, 1), act)()

            @pl.when(l != c)
            def _():
                for i, (dz, ok) in enumerate(((1, z < 3), (-1, z > 0))):
                    @pl.when(ok)
                    def _():
                        for j, xq in enumerate((x, 1 - x)):
                            getattr(copy_to(xq, z + dz, 2 * i + j), act)()

    def wait_piece(what, p):
        reg = region(what, c, p)
        remote(reg, reg, sib_s.at[what, p], piece_r.at[what, p], sibling).wait_recv()

    def far_copy(what, p, i):
        reg = region(what, c, p)
        return remote(reg, reg, far_s.at[what, i], piece_r.at[what, p], at(x, y, far, c))

    def y_copy(what, p, i):
        reg = region(what, c, p)
        return remote(reg, reg, y_s.at[what, i], piece_r.at[what, p], at(x, 1 - y, z, c))

    def sib_copy(what, p):
        reg = region(what, c, p)
        return remote(reg, reg, sib_s.at[what, p], sib_r.at[what, p], sibling)

    def piece(slot, dx, dy=0):
        return 4 * planes[slot] + 2 * (1 - y if dy else y) + (1 - x if dx else x)

    def relay(what, slot, dx):
        p = piece(slot, dx)
        if slot == 0 and dx == 0:
            @pl.when(c == l)
            def _():
                pltpu.make_async_copy(
                    source(what, 0, x), region(what, c, p), local_sem.at[what]
                ).wait()

            @pl.when(c != l)
            def _():
                wait_piece(what, p)
        else:
            wait_piece(what, p)
        if slot == 0:
            far_copy(what, p, dx).start()
        if slot == 3:
            @pl.when(inner)
            def _():
                far_copy(what, p, 2 + dx).start()
        y_copy(what, p, 2 * slot + dx).start()
        sib_copy(what, p).start()

    def relay_both(what, slot):
        for dx in range(2):
            relay(what, slot, dx)

    def relay_y(what, slot):
        for dx in range(2):
            p = piece(slot, dx, 1)
            wait_piece(what, p)
            sib_copy(what, p).start()

    def wait_sib(what, slot):
        for dy in range(2):
            for dx in range(2):
                p = piece(slot, dx, dy)
                reg = region(what, 1 - c, p)
                remote(reg, reg, sib_s.at[what, p], sib_r.at[what, p], sibling).wait_recv()

    own_rows = pl.ds(pl.multiple_of(c * half, half), half)
    sib_rows = pl.ds(pl.multiple_of((1 - c) * half, half), half)
    loads = [
        pltpu.make_async_copy(q_hbm, qbuf, load_sem.at[0]),
        pltpu.make_async_copy(k_hbm, kbuf.at[pl.ds(WINDOW, rows)], load_sem.at[1]),
        pltpu.make_async_copy(v_hbm, vbuf.at[pl.ds(WINDOW, rows)], load_sem.at[2]),
        pltpu.make_async_copy(docs_hbm, dbuf.at[pl.ds(1, blocks)], load_sem.at[3]),
        pltpu.make_async_copy(ow_hbm, ow, load_sem.at[4]),
        pltpu.make_async_copy(res_hbm.at[own_rows], res, load_sem.at[5]),
    ]
    for load in loads:
        load.start()

    tail = pl.ds(rows - WINDOW, WINDOW)
    head = pl.ds(0, WINDOW)
    after = {"sp": lax.rem(sp + 1, n_sp), "tp": c}

    halo = [
        remote(k_hbm.at[tail], kbuf.at[head], halo_s.at[0], halo_r.at[0], after),
        remote(v_hbm.at[tail], vbuf.at[head], halo_s.at[1], halo_r.at[1], after),
        remote(docs_hbm.at[blocks - 1], dbuf.at[0], halo_s.at[2], halo_r.at[2], after),
    ]

    @pl.when(sp < n_sp - 1)
    def _():
        for copy in halo:
            copy.start()

    first_sends(GATE_UP, "start")
    relay(GATE_UP, 0, 0)

    @pl.when(sp == 0)
    def _():
        kbuf[head, :] = jnp.zeros((WINDOW, kbuf.shape[1]), kbuf.dtype)
        vbuf[head, :] = jnp.zeros((WINDOW, vbuf.shape[1]), vbuf.dtype)
        dbuf[0] = jnp.full((1, WINDOW), -1, jnp.int32)

    for load in loads[:4]:
        load.wait()

    def attend_block(n):
        at_rows = pl.ds(pl.multiple_of(n * WINDOW, WINDOW), WINDOW)
        band = pl.ds(pl.multiple_of(n * WINDOW, WINDOW), 2 * WINDOW)
        before_docs, here_docs = dbuf[n], dbuf[n + 1]
        query_docs = jnp.transpose(jnp.broadcast_to(here_docs, (WINDOW, WINDOW)))
        row = lax.broadcasted_iota(jnp.int32, (WINDOW, WINDOW), 0)
        col = lax.broadcasted_iota(jnp.int32, (WINDOW, WINDOW), 1)
        left = (col > row) & (query_docs == before_docs)
        right = (col <= row) & (query_docs == here_docs)
        allowed = jnp.concatenate([left.astype(jnp.int32), right.astype(jnp.int32)], axis=1)
        allowed = jnp.concatenate([allowed] * per_kv, axis=0) != 0
        for j in range(kv_local):
            keys = kbuf[band, j * HD : (j + 1) * HD]
            vals = vbuf[band, j * HD : (j + 1) * HD]
            wide = qbuf[at_rows, j * per_kv * HD : (j + 1) * per_kv * HD]
            query = jnp.concatenate([wide[:, h * HD : (h + 1) * HD] for h in range(per_kv)], axis=0)
            scores = lax.dot_general(
                query, keys, (((1,), (1,)), ((), ())), preferred_element_type=jnp.float32
            ) * HD ** (-0.5)
            scores = jnp.where(allowed, scores, -1e30)
            sink = jnp.concatenate(
                [jnp.full((WINDOW, 1), sink_ref[j * per_kv + h], jnp.float32) for h in range(per_kv)],
                axis=0,
            )
            peak = jnp.maximum(jnp.max(scores, axis=-1, keepdims=True), sink)
            raised = jnp.exp(scores - peak)
            denom = jnp.sum(raised, axis=-1, keepdims=True) + jnp.exp(sink - peak)
            weights = (raised * (1.0 / denom)).astype(jnp.bfloat16)
            mixed = jnp.dot(weights, vals, preferred_element_type=jnp.float32)
            mixed = jnp.concatenate(
                [mixed[h * WINDOW : (h + 1) * WINDOW] for h in range(per_kv)], axis=1
            )
            att[at_rows, j * per_kv * HD : (j + 1) * per_kv * HD] = mixed.astype(jnp.bfloat16)

    def attend_loop(n, carry):
        attend_block(n)
        return carry

    lax.fori_loop(1, blocks, attend_loop, 0)

    @pl.when(sp > 0)
    def _():
        for copy in halo:
            copy.wait_recv()

    lax.fori_loop(0, 1, attend_loop, 0)
    loads[4].wait()

    def project(at_rows, dst):
        def body(i, carry):
            cols = pl.ds(pl.multiple_of(i * 256, 256), 256)
            dst[:, cols] = jnp.dot(
                att[at_rows, :], ow[:, cols], preferred_element_type=jnp.float32
            ).astype(jnp.bfloat16)
            return carry

        lax.fori_loop(0, width // 256, body, 0)

    project(sib_rows, mix_out)
    mix_copy = remote(mix_out, mix_in, mix_s, mix_r, sibling)
    mix_copy.start()
    project(own_rows, mix_own)
    loads[5].wait()
    mix_copy.wait_recv()

    base = 3 * half

    def norm_body(i, carry):
        at_rows = pl.ds(pl.multiple_of(i * 32, 32), 32)
        mixed = mix_own[at_rows, :].astype(jnp.float32) + mix_in[at_rows, :].astype(jnp.float32)
        stream = (res[at_rows, :].astype(jnp.float32) + mixed).astype(jnp.bfloat16)
        res[at_rows, :] = stream
        floats = stream.astype(jnp.float32)
        scale = lax.rsqrt(jnp.mean(floats * floats, axis=-1, keepdims=True) + 1e-06)
        xbuf[pl.ds(pl.multiple_of(base + i * 32, 32), 32), :] = (
            floats * scale * gain_ref[...]
        ).astype(jnp.bfloat16)
        return carry

    chunk = half // 2

    def rows_of(block, i):
        return xbuf.at[pl.ds(block * half + i * chunk, chunk)]

    def token_copy(kind, i):
        src, dst, dev = {
            0: (2, 0, x_peer),
            1: (3, 1, x_peer),
            2: (3, 2, z_peer),
        }[kind]
        return remote(
            rows_of(src, i), rows_of(dst, i), tok_s.at[kind, i], tok_r.at[kind, i], dev
        )

    relay(GATE_UP, 0, 1)
    for i in range(2):
        lax.fori_loop(i * (chunk // 32), (i + 1) * (chunk // 32), norm_body, 0)
        token_copy(1, i).start()
        token_copy(2, i).start()

    @pl.when(inner)
    def _():
        relay_both(GATE_UP, 3)

    relay_both(GATE_UP, 1)
    relay_y(GATE_UP, 0)
    for i in range(2):
        token_copy(2, i).wait_recv()
        token_copy(0, i).start()
    first_sends(DOWN, "start")
    relay(DOWN, 0, 0)
    relay_both(GATE_UP, 2)

    @pl.when(outer)
    def _():
        relay_both(GATE_UP, 3)

    for slot in (1, 3, 2):
        relay_y(GATE_UP, slot)
    relay(DOWN, 0, 1)
    for slot in range(4):
        wait_sib(GATE_UP, slot)
    for i in range(2):
        token_copy(1, i).wait_recv()
        token_copy(0, i).wait_recv()

    pair = 2 * half

    def gate_up(which, lo, hi):
        at_rows = pl.ds(which * pair, pair)

        def body(i, carry):
            cols = pl.ds(pl.multiple_of(i * 256, 256), 256)
            acts[:, cols] = jnp.dot(
                xbuf[at_rows, :], wgu[:, cols], preferred_element_type=jnp.float32
            )
            return carry

        lax.fori_loop(lo, hi, body, 0)

    def activate(which):
        def body(i, carry):
            at_rows = pl.ds(pl.multiple_of(i * 32, 32), 32)
            gate, up = acts[at_rows, :units], acts[at_rows, units:]
            hid[pl.ds(pl.multiple_of(which * pair + i * 32, 32), 32), :] = (
                gate / (1.0 + jnp.exp(-gate)) * up
            ).astype(jnp.bfloat16)
            return carry

        lax.fori_loop(0, pair // 32, body, 0)

    def slab_cols(slot):
        return pl.ds(pl.multiple_of(planes[slot] * slab, slab), slab)

    def x_copy(slot):
        part = pbuf.at[:, slab_cols(slot)]
        return remote(part, rx.at[:, slab_cols(slot)], rx_s.at[planes[slot]], rx_r.at[planes[slot]], x_peer)

    def z_copy(slot):
        part = zbuf.at[:, slab_cols(slot)]
        return remote(part, rz.at[:, slab_cols(slot)], rz_s.at[planes[slot]], rz_r.at[planes[slot]], z_peer)

    def out_copy(slot):
        part = obuf.at[:, slab_cols(slot)]
        dst = o_hbm.at[own_rows, slab_cols(slot)]
        i = planes[slot]
        return (
            pltpu.make_async_copy(part, dst, out_l.at[i]),
            remote(part, dst, out_s.at[i], out_r.at[i], sibling),
        )

    def down_first(slot):
        def body(i, carry):
            cols = pl.ds(pl.multiple_of(planes[slot] * slab + i * 256, 256), 256)
            pbuf[:, cols] = jnp.dot(
                hid[:pair, :], wd[:, cols], preferred_element_type=jnp.float32
            ).astype(jnp.bfloat16)
            return carry

        lax.fori_loop(0, slab // 256, body, 0)
        x_copy(slot).start()

    def down_second(slot):
        def body(i, carry):
            cols = pl.ds(pl.multiple_of(planes[slot] * slab + i * 256, 256), 256)
            part = jnp.dot(hid[pair:, :], wd[:, cols], preferred_element_type=jnp.float32)
            zbuf[:, cols] = part[:half].astype(jnp.bfloat16)
            own[:, cols] = part[half:]
            return carry

        lax.fori_loop(0, slab // 256, body, 0)

    def combine(slot):
        x_copy(slot).wait_recv()

        def body(i, carry):
            cols = pl.ds(pl.multiple_of(planes[slot] * slab + i * 256, 256), 256)
            zbuf[:, cols] = (
                zbuf[:, cols].astype(jnp.float32) + rx[:half, cols].astype(jnp.float32)
            ).astype(jnp.bfloat16)
            return carry

        lax.fori_loop(0, slab // 256, body, 0)
        z_copy(slot).start()

    def finish(slot):
        z_copy(slot).wait_recv()

        def body(i, carry):
            cols = pl.ds(pl.multiple_of(planes[slot] * slab + i * 256, 256), 256)
            total = own[:, cols] + rx[half:, cols].astype(jnp.float32) + rz[:, cols].astype(jnp.float32)
            obuf[:, cols] = (res[:, cols].astype(jnp.float32) + total).astype(jnp.bfloat16)
            return carry

        lax.fori_loop(0, slab // 256, body, 0)
        for copy in out_copy(slot):
            copy.start()

    n_cols = 2 * units // 256
    gate_up(0, 0, n_cols // 2)

    @pl.when(inner)
    def _():
        relay_both(DOWN, 3)

    relay_both(DOWN, 1)
    gate_up(0, n_cols // 2, n_cols)
    activate(0)
    relay_y(DOWN, 0)
    relay_y(DOWN, 1)
    for slot in (0, 1):
        wait_sib(DOWN, slot)
        down_first(slot)
    relay_both(DOWN, 2)

    @pl.when(outer)
    def _():
        relay_both(DOWN, 3)

    gate_up(1, 0, n_cols)
    activate(1)
    for slot in (3, 2):
        relay_y(DOWN, slot)
    for slot in (0, 1):
        down_second(slot)
    for slot in (3, 2):
        wait_sib(DOWN, slot)
        down_first(slot)
    for slot in (0, 1):
        combine(slot)
    for slot in (3, 2):
        down_second(slot)
        combine(slot)
    for slot in (0, 1, 3, 2):
        finish(slot)

    for slot in range(4):
        here, there = out_copy(slot)
        here.wait()
        there.wait()
        x_copy(slot).wait_send()
        z_copy(slot).wait_send()

    @pl.when(sp < n_sp - 1)
    def _():
        for copy in halo:
            copy.wait_send()

    mix_copy.wait_send()
    for kind in range(3):
        for i in range(2):
            token_copy(kind, i).wait_send()
    for what in (GATE_UP, DOWN):
        first_sends(what, "wait_send")
        for slot in range(4):
            for dx in range(2):
                p = piece(slot, dx)
                y_copy(what, p, 2 * slot + dx).wait_send()
                for dy in range(2):
                    sib_copy(what, piece(slot, dx, dy)).wait_send()
        for dx in range(2):
            far_copy(what, piece(0, dx), dx).wait_send()

            @pl.when(inner)
            def _():
                far_copy(what, piece(3, dx), 2 + dx).wait_send()


def fused_on_device(
    queries, key_rows, values, doc_ids, sink_logits, residual, out_weight, norm_gain, w_gate, w_up, w_down
):
    rows, width = residual.shape
    half = rows // 2
    units = w_gate.shape[1] // 2
    pieces = lax.axis_size("sp")
    bf16, f32 = jnp.bfloat16, jnp.float32
    anywhere = pl.BlockSpec(memory_space=pl.ANY)
    dma = pltpu.SemaphoreType.DMA
    docs = doc_ids.reshape(rows // WINDOW, 1, WINDOW)
    return pl.pallas_call(
        layer_kernel,
        out_shape=jax.ShapeDtypeStruct((rows, width), bf16),
        in_specs=[
            anywhere, anywhere, anywhere, anywhere,
            pl.BlockSpec(memory_space=pltpu.SMEM),
            anywhere, anywhere,
            pl.BlockSpec(memory_space=pltpu.VMEM),
            anywhere, anywhere, anywhere,
        ],
        out_specs=anywhere,
        scratch_shapes=[
            pltpu.VMEM((width, 2 * units), bf16),
            pltpu.VMEM((units, width), bf16),
            pltpu.VMEM((4 * half, width), bf16),
            pltpu.VMEM((2 * half, 2 * units), f32),
            pltpu.VMEM((4 * half, units), bf16),
            pltpu.VMEM((2 * half, width), bf16),
            pltpu.VMEM((half, width), bf16),
            pltpu.VMEM((2 * half, width), bf16),
            pltpu.VMEM((half, width), bf16),
            pltpu.VMEM((half, width), f32),
            pltpu.VMEM(queries.shape, bf16),
            pltpu.VMEM((rows + WINDOW, key_rows.shape[1]), bf16),
            pltpu.VMEM((rows + WINDOW, key_rows.shape[1]), bf16),
            pltpu.VMEM((rows // WINDOW + 1, 1, WINDOW), jnp.int32),
            pltpu.VMEM(queries.shape, bf16),
            pltpu.VMEM(out_weight.shape, bf16),
            pltpu.VMEM((half, width), bf16),
            pltpu.VMEM((half, width), bf16),
            pltpu.VMEM((half, width), bf16),
            pltpu.VMEM((half, width), bf16),
            pltpu.VMEM((half, width), bf16),
            dma((6,)), dma((3,)), dma((3,)), dma((2, 2, 4)), dma((2,)), dma((2, 4)), dma((2, 8)),
            dma((2, pieces)), dma((2, pieces)), dma((2, pieces)),
            dma, dma, dma((3, 2)), dma((3, 2)), dma((4,)), dma((4,)), dma((4,)), dma((4,)),
            dma((4,)), dma((4,)), dma((4,)),
        ],
        compiler_params=pltpu.CompilerParams(has_side_effects=True, vmem_limit_bytes=63 * 2**20),
        name="layer",
    )(
        queries, key_rows, values, docs, sink_logits, residual, out_weight,
        norm_gain.reshape(1, width), w_gate, w_up, w_down,
    )


def solution(mesh):
    if (mesh.shape["sp"], mesh.shape["tp"]) != (16, 2):
        return staged_solution(mesh)
    in_specs = (
        P("sp", "tp"), P("sp", "tp"), P("sp", "tp"), P("sp"), P("tp"), P("sp", None), P("tp", None),
        P(), P("sp", "tp"), P("sp", "tp"), P("tp", "sp"),
    )
    return jax.shard_map(
        fused_on_device, mesh=mesh, in_specs=in_specs, out_specs=P("sp", None), check_vma=False
    )
```

profile of v0, /device:TPU:17, one launch (start us, length us, event | category | flops | bytes accessed | tf_op | source)
XLA Modules:
  0.0 198.3 jit_solution(9975621238566906448)
XLA Ops:
  0.0 195.1 %layer.1 = bf16[512,2048]{1,0:T(8,128)(2,1)} custom-call(bf16[512,512]{1,0:T(8,128)(2,1)} %q_hbm.1, bf16[512,256]{1,0:T(8,128)(2,1)} %k_hbm.1, bf16[512,256]{1,0:T(8,128)(2,1)} %v_hbm.1, s32[4,1,128]{2,1,0:T(1,128)} %bitcast.3, f32[8]{0:T(128)} %sink_ref.1, bf16[512,2048]{1,0:T(8,128)(2,1)} %res_hbm.1, bf16[512,2048]{1,0:T(8,128)(2,1)} %ow_hbm.1, ...), custom_call_target="tpu_custom_call" | custom-call | tf_op jit(solution)/shard_map/layer/pallas_call | solution.py:690
  195.1 3.2 %copy.13 = bf16[512,2048]{1,0:T(8,128)(2,1)} copy(bf16[512,2048]{1,0:T(8,128)(2,1)} %layer.1) | data formatting | bytes 4194304
where the time goes:
time: 198 us
  Pallas kernels  195 us (98%)
  local copies, waits for them, and re-layouts  3.16 us (2%)
    pallas_call x1, Pallas kernels, fused_on_device(): pl.pallas_call(layer_kernel, out_shape=jax.ShapeDtypeStruct((rows, width)...  195 us

commit v1 on v0

--- a/solution.py
+++ b/solution.py
@@ -220,8 +220,21 @@
     x, y, z = lax.rem(sp, 2), lax.rem(lax.div(sp, 2), 2), lax.div(sp, 4)
     l, h = lax.rem(z, 2), lax.div(z, 2)
     far, near = 2 * (1 - h) + l, 2 * h + 1 - l
-    inner, outer = z * (3 - z) == 2, z * (3 - z) == 0
-    planes = (z, z + 1 - 2 * h, far, 3 * (1 - l))
+    mid = lax.div(z * (3 - z), 2)
+    inner, outer = mid == 1, mid == 0
+    toward, edge = z + 1 - 2 * h, 3 * (1 - l)
+    planes = (
+        z,
+        mid * edge + (1 - mid) * toward,
+        far,
+        mid * toward + (1 - mid) * edge,
+    )
+    down_planes = (
+        planes[0],
+        planes[1],
+        mid * toward + (1 - mid) * far,
+        mid * far + (1 - mid) * edge,
+    )
     depth, units = gate_hbm.shape[0], gate_hbm.shape[1] // 2
     half_units = units // 2
     rows, width = res_hbm.shape
@@ -258,16 +271,17 @@
             return (gate_hbm, up_hbm)[k].at[:, pl.ds(pl.multiple_of(xq * units, 128), units)]
         return down_hbm.at[pl.ds(pl.multiple_of(xq * units + k * half_units, 16), half_units), :]
 
-    def first_sends(what, act):
-        for k in range(2):
-            def copy_to(xq, z_, slot):
-                return remote(
-                    source(what, k, xq), region(what, k, sp), first_s.at[what, k, slot],
-                    piece_r.at[what, sp], at(xq, y, z_, k),
-                )
-
-            @pl.when(l == c)
-            def _():
+    def first_sends(what, act, plane):
+        def copy_to(k, xq, z_, slot):
+            return remote(
+                source(what, k, xq), region(what, k, sp), first_s.at[what, k, slot],
+                piece_r.at[what, sp], at(xq, y, z_, k),
+            )
+
+        def within():
+            for k in range(2):
+                getattr(copy_to(k, 1 - x, z, 1), act)()
+
                 @pl.when(c == k)
                 def _():
                     if act == "start":
@@ -277,17 +291,22 @@
 
                 @pl.when(c != k)
                 def _():
-                    getattr(copy_to(x, z, 0), act)()
-
-                getattr(copy_to(1 - x, z, 1), act)()
-
-            @pl.when(l != c)
+                    getattr(copy_to(k, x, z, 0), act)()
+
+        def across(away, j):
+            xq, to = (1 - x if j else x), (2 * z - toward if away else toward)
+            for k in range(2):
+                getattr(copy_to(k, xq, to, 2 * away + j), act)()
+
+        if plane == "own":
+            pl.when(l == c)(within)
+        elif plane == "away":
+            @pl.when(jnp.logical_and(l != c, inner))
             def _():
-                for i, (dz, ok) in enumerate(((1, z < 3), (-1, z > 0))):
-                    @pl.when(ok)
-                    def _():
-                        for j, xq in enumerate((x, 1 - x)):
-                            getattr(copy_to(xq, z + dz, 2 * i + j), act)()
+                across(1, 0)
+                across(1, 1)
+        else:
+            pl.when(l != c)(lambda: across(0, plane == "toward_crossing"))
 
     def wait_piece(what, p):
         reg = region(what, c, p)
@@ -305,11 +324,11 @@
         reg = region(what, c, p)
         return remote(reg, reg, sib_s.at[what, p], sib_r.at[what, p], sibling)
 
-    def piece(slot, dx, dy=0):
-        return 4 * planes[slot] + 2 * (1 - y if dy else y) + (1 - x if dx else x)
-
-    def relay(what, slot, dx):
-        p = piece(slot, dx)
+    def piece(what, slot, dx, dy=0):
+        return 4 * (planes, down_planes)[what][slot] + 2 * (1 - y if dy else y) + (1 - x if dx else x)
+
+    def relay(what, slot, dx, onward=True):
+        p = piece(what, slot, dx)
         if slot == 0 and dx == 0:
             @pl.when(c == l)
             def _():
@@ -322,9 +341,9 @@
                 wait_piece(what, p)
         else:
             wait_piece(what, p)
-        if slot == 0:
+        if slot == 0 and onward:
             far_copy(what, p, dx).start()
-        if slot == 3:
+        if slot == 1:
             @pl.when(inner)
             def _():
                 far_copy(what, p, 2 + dx).start()
@@ -337,16 +356,35 @@
 
     def relay_y(what, slot):
         for dx in range(2):
-            p = piece(slot, dx, 1)
+            p = piece(what, slot, dx, 1)
             wait_piece(what, p)
             sib_copy(what, p).start()
 
     def wait_sib(what, slot):
         for dy in range(2):
             for dx in range(2):
-                p = piece(slot, dx, dy)
+                p = piece(what, slot, dx, dy)
                 reg = region(what, 1 - c, p)
                 remote(reg, reg, sib_s.at[what, p], sib_r.at[what, p], sibling).wait_recv()
+
+    greeted = [
+        (sibling, None), (at(x, 1 - y, z, c), None), (at(x, y, far, c), None),
+        (at(1 - x, y, z, 0), None), (at(1 - x, y, z, 1), None),
+        ({"sp": lax.rem(sp + 1, n_sp), "tp": c}, sp < n_sp - 1),
+        ({"sp": lax.rem(sp + n_sp - 1, n_sp), "tp": c}, sp > 0),
+    ]
+    for dz, ok in ((1, z < 3), (-1, z > 0)):
+        greeted += [(at(x_, y, z + dz, c_), ok) for x_ in (x, 1 - x) for c_ in range(2)]
+    barrier = pltpu.get_barrier_semaphore()
+    for dev, ok in greeted:
+        def greet():
+            pl.semaphore_signal(barrier, inc=1, device_id=dev, device_id_type=MESH)
+
+        if ok is None:
+            greet()
+        else:
+            pl.when(ok)(greet)
+    pl.semaphore_wait(barrier, sum(1 if ok is None else ok.astype(jnp.int32) * 1 for _, ok in greeted))
 
     own_rows = pl.ds(pl.multiple_of(c * half, half), half)
     sib_rows = pl.ds(pl.multiple_of((1 - c) * half, half), half)
@@ -376,7 +414,14 @@
         for copy in halo:
             copy.start()
 
-    first_sends(GATE_UP, "start")
+    first_sends(GATE_UP, "start", "own")
+    first_sends(GATE_UP, "start", "away")
+
+    @pl.when(outer)
+    def _():
+        first_sends(GATE_UP, "start", "toward")
+        first_sends(GATE_UP, "start", "toward_crossing")
+
     relay(GATE_UP, 0, 0)
 
     @pl.when(sp == 0)
@@ -427,6 +472,14 @@
         return carry
 
     lax.fori_loop(1, blocks, attend_loop, 0)
+    relay(GATE_UP, 0, 1)
+
+    @pl.when(inner)
+    def _():
+        first_sends(GATE_UP, "start", "toward_crossing")
+        first_sends(GATE_UP, "start", "toward")
+
+    first_sends(DOWN, "start", "own")
 
     @pl.when(sp > 0)
     def _():
@@ -453,7 +506,7 @@
     loads[5].wait()
     mix_copy.wait_recv()
 
-    base = 3 * half
+    base = half
 
     def norm_body(i, carry):
         at_rows = pl.ds(pl.multiple_of(i * 32, 32), 32)
@@ -474,181 +527,262 @@
 
     def token_copy(kind, i):
         src, dst, dev = {
-            0: (2, 0, x_peer),
-            1: (3, 1, x_peer),
-            2: (3, 2, z_peer),
+            0: (3, 2, x_peer),
+            1: (1, 0, x_peer),
+            2: (1, 3, z_peer),
+            3: (0, 2, z_peer),
         }[kind]
         return remote(
             rows_of(src, i), rows_of(dst, i), tok_s.at[kind, i], tok_r.at[kind, i], dev
         )
 
-    relay(GATE_UP, 0, 1)
-    for i in range(2):
-        lax.fori_loop(i * (chunk // 32), (i + 1) * (chunk // 32), norm_body, 0)
-        token_copy(1, i).start()
-        token_copy(2, i).start()
-
-    @pl.when(inner)
-    def _():
-        relay_both(GATE_UP, 3)
-
-    relay_both(GATE_UP, 1)
-    relay_y(GATE_UP, 0)
-    for i in range(2):
-        token_copy(2, i).wait_recv()
-        token_copy(0, i).start()
-    first_sends(DOWN, "start")
-    relay(DOWN, 0, 0)
-    relay_both(GATE_UP, 2)
-
-    @pl.when(outer)
-    def _():
-        relay_both(GATE_UP, 3)
-
-    for slot in (1, 3, 2):
-        relay_y(GATE_UP, slot)
-    relay(DOWN, 0, 1)
-    for slot in range(4):
-        wait_sib(GATE_UP, slot)
-    for i in range(2):
-        token_copy(1, i).wait_recv()
-        token_copy(0, i).wait_recv()
-
     pair = 2 * half
 
-    def gate_up(which, lo, hi):
+    def gate_up(which, slot):
         at_rows = pl.ds(which * pair, pair)
+        depths = pl.ds(pl.multiple_of(planes[slot] * slab, slab), slab)
 
         def body(i, carry):
             cols = pl.ds(pl.multiple_of(i * 256, 256), 256)
-            acts[:, cols] = jnp.dot(
+            part = jnp.dot(
+                xbuf[at_rows, depths], wgu[depths, cols], preferred_element_type=jnp.float32
+            )
+            acts[at_rows, cols] = part if slot == 0 else acts[at_rows, cols] + part
+            return carry
+
+        lax.fori_loop(0, 2 * units // 256, body, 0)
+
+    def gate_up_whole(which, low, high):
+        at_rows = pl.ds(which * pair, pair)
+
+        def body(i, carry):
+            cols = pl.ds(pl.multiple_of(i * 256, 256), 256)
+            acts[at_rows, cols] = jnp.dot(
                 xbuf[at_rows, :], wgu[:, cols], preferred_element_type=jnp.float32
             )
             return carry
 
-        lax.fori_loop(lo, hi, body, 0)
+        lax.fori_loop(low, high, body, 0)
 
     def activate(which):
         def body(i, carry):
-            at_rows = pl.ds(pl.multiple_of(i * 32, 32), 32)
+            at_rows = pl.ds(pl.multiple_of(which * pair + i * 32, 32), 32)
             gate, up = acts[at_rows, :units], acts[at_rows, units:]
-            hid[pl.ds(pl.multiple_of(which * pair + i * 32, 32), 32), :] = (
-                gate / (1.0 + jnp.exp(-gate)) * up
-            ).astype(jnp.bfloat16)
+            hid[at_rows, :] = (gate / (1.0 + jnp.exp(-gate)) * up).astype(jnp.bfloat16)
             return carry
 
         lax.fori_loop(0, pair // 32, body, 0)
 
     def slab_cols(slot):
-        return pl.ds(pl.multiple_of(planes[slot] * slab, slab), slab)
-
-    def x_copy(slot):
-        part = pbuf.at[:, slab_cols(slot)]
-        return remote(part, rx.at[:, slab_cols(slot)], rx_s.at[planes[slot]], rx_r.at[planes[slot]], x_peer)
+        return pl.ds(pl.multiple_of(down_planes[slot] * slab, slab), slab)
+
+    def x_copy(part, slot):
+        i, cols = down_planes[slot], slab_cols(slot)
+        dev = z_peer if (part, slot) == (0, 3) else x_peer
+        return remote(
+            pbuf.at[part, :, cols], rx.at[part, :, cols], rx_s.at[part, i], rx_r.at[part, i], dev
+        )
 
     def z_copy(slot):
-        part = zbuf.at[:, slab_cols(slot)]
-        return remote(part, rz.at[:, slab_cols(slot)], rz_s.at[planes[slot]], rz_r.at[planes[slot]], z_peer)
+        i, cols = down_planes[slot], slab_cols(slot)
+        return remote(zbuf.at[:, cols], rz.at[:, cols], rz_s.at[i], rz_r.at[i], z_peer)
 
     def out_copy(slot):
-        part = obuf.at[:, slab_cols(slot)]
+        part, i = obuf.at[:, slab_cols(slot)], down_planes[slot]
         dst = o_hbm.at[own_rows, slab_cols(slot)]
-        i = planes[slot]
         return (
             pltpu.make_async_copy(part, dst, out_l.at[i]),
             remote(part, dst, out_s.at[i], out_r.at[i], sibling),
         )
 
+    def over_columns(slot, step):
+        def body(i, carry):
+            step(pl.ds(pl.multiple_of(down_planes[slot] * slab + i * 256, 256), 256))
+            return carry
+
+        lax.fori_loop(0, slab // 256, body, 0)
+
     def down_first(slot):
-        def body(i, carry):
-            cols = pl.ds(pl.multiple_of(planes[slot] * slab + i * 256, 256), 256)
-            pbuf[:, cols] = jnp.dot(
-                hid[:pair, :], wd[:, cols], preferred_element_type=jnp.float32
+        def step(cols):
+            part = jnp.dot(hid[:pair, :], wd[:, cols], preferred_element_type=jnp.float32)
+            pbuf[1, :, cols] = part[:half].astype(jnp.bfloat16)
+            own[:, cols] = part[half:]
+
+        over_columns(slot, step)
+        if slot < 3:
+            x_copy(1, slot).start()
+
+    def down_second(slot):
+        def step(cols):
+            part = jnp.dot(hid[pair:, :], wd[:, cols], preferred_element_type=jnp.float32)
+            pbuf[0, :, cols] = part[:half].astype(jnp.bfloat16)
+            zbuf[:, cols] = part[half:].astype(jnp.bfloat16)
+
+        over_columns(slot, step)
+        x_copy(0, slot).start()
+        if slot == 3:
+            z_copy(slot).start()
+
+    def combine(slot):
+        x_copy(0, slot).wait_recv()
+
+        def step(cols):
+            mine = zbuf if slot < 3 else pbuf.at[1]
+            mine[:, cols] = (
+                mine[:, cols].astype(jnp.float32) + rx[0, :, cols].astype(jnp.float32)
             ).astype(jnp.bfloat16)
-            return carry
-
-        lax.fori_loop(0, slab // 256, body, 0)
-        x_copy(slot).start()
-
-    def down_second(slot):
-        def body(i, carry):
-            cols = pl.ds(pl.multiple_of(planes[slot] * slab + i * 256, 256), 256)
-            part = jnp.dot(hid[pair:, :], wd[:, cols], preferred_element_type=jnp.float32)
-            zbuf[:, cols] = part[:half].astype(jnp.bfloat16)
-            own[:, cols] = part[half:]
-            return carry
-
-        lax.fori_loop(0, slab // 256, body, 0)
-
-    def combine(slot):
-        x_copy(slot).wait_recv()
-
-        def body(i, carry):
-            cols = pl.ds(pl.multiple_of(planes[slot] * slab + i * 256, 256), 256)
-            zbuf[:, cols] = (
-                zbuf[:, cols].astype(jnp.float32) + rx[:half, cols].astype(jnp.float32)
-            ).astype(jnp.bfloat16)
-            return carry
-
-        lax.fori_loop(0, slab // 256, body, 0)
-        z_copy(slot).start()
+
+        over_columns(slot, step)
+        (z_copy(slot) if slot < 3 else x_copy(1, slot)).start()
 
     def finish(slot):
+        x_copy(1, slot).wait_recv()
         z_copy(slot).wait_recv()
 
-        def body(i, carry):
-            cols = pl.ds(pl.multiple_of(planes[slot] * slab + i * 256, 256), 256)
-            total = own[:, cols] + rx[half:, cols].astype(jnp.float32) + rz[:, cols].astype(jnp.float32)
+        def step(cols):
+            total = own[:, cols] + rx[1, :, cols].astype(jnp.float32) + rz[:, cols].astype(jnp.float32)
             obuf[:, cols] = (res[:, cols].astype(jnp.float32) + total).astype(jnp.bfloat16)
-            return carry
-
-        lax.fori_loop(0, slab // 256, body, 0)
+
+        over_columns(slot, step)
         for copy in out_copy(slot):
             copy.start()
 
-    n_cols = 2 * units // 256
-    gate_up(0, 0, n_cols // 2)
+    def forward_tokens(i, kind):
+        token_copy(1 if kind == 3 else 2, i).wait_recv()
+        token_copy(kind, i).start()
+
+    def await_tokens(kind):
+        for i in range(2):
+            token_copy(kind, i).wait_recv()
+
+    def await_diagonal():
+        @pl.when(outer)
+        def _():
+            await_tokens(0)
+
+        @pl.when(inner)
+        def _():
+            await_tokens(2)
+            await_tokens(3)
+
+    def send_tokens(kind, i):
+        token_copy(kind, i).start()
+
+    for i in range(2):
+        lax.fori_loop(i * (chunk // 32), (i + 1) * (chunk // 32), norm_body, 0)
+        token_copy(1, i).start()
+
+    @pl.when(outer)
+    def _():
+        send_tokens(2, 0)
+        send_tokens(2, 1)
+
+    relay(DOWN, 0, 0, onward=False)
+
+    @pl.when(outer)
+    def _():
+        relay(DOWN, 0, 1, onward=False)
+        relay_both(GATE_UP, 2)
+
+    relay_y(GATE_UP, 0)
+    relay_both(GATE_UP, 1)
 
     @pl.when(inner)
     def _():
-        relay_both(DOWN, 3)
-
-    relay_both(DOWN, 1)
-    gate_up(0, n_cols // 2, n_cols)
+        send_tokens(2, 0)
+        relay_both(GATE_UP, 2)
+        relay_y(GATE_UP, 1)
+        relay(GATE_UP, 3, 1)
+        send_tokens(2, 1)
+        relay(DOWN, 0, 1, onward=False)
+        await_tokens(1)
+
+    @pl.when(outer)
+    def _():
+        relay_y(GATE_UP, 2)
+        for plane in ("toward_crossing", "toward"):
+            first_sends(DOWN, "start", plane)
+        forward_tokens(0, 3)
+        forward_tokens(1, 3)
+        forward_tokens(0, 0)
+        relay_y(GATE_UP, 1)
+        relay(GATE_UP, 3, 0)
+        relay(GATE_UP, 3, 1)
+
+    wait_sib(GATE_UP, 0)
+    gate_up(0, 0)
+
+    @pl.when(inner)
+    def _():
+        relay(GATE_UP, 3, 0)
+        relay_y(GATE_UP, 2)
+        for plane in ("toward_crossing", "toward"):
+            first_sends(DOWN, "start", plane)
+
+    @pl.when(outer)
+    def _():
+        forward_tokens(1, 0)
+
+    wait_sib(GATE_UP, 1)
+    gate_up(0, 1)
+    wait_sib(GATE_UP, 2)
+    gate_up(0, 2)
+    first_sends(DOWN, "start", "away")
+    for dx in range(2):
+        far_copy(DOWN, piece(DOWN, 0, dx), dx).start()
+
+    @pl.when(inner)
+    def _():
+        relay_both(DOWN, 1)
+
+    relay_y(GATE_UP, 3)
+    relay_y(DOWN, 0)
+    wait_sib(GATE_UP, 3)
+    gate_up(0, 3)
     activate(0)
-    relay_y(DOWN, 0)
+    wait_sib(DOWN, 0)
+    down_first(0)
+
+    @pl.when(outer)
+    def _():
+        relay_both(DOWN, 1)
+        relay_both(DOWN, 2)
+
+    await_diagonal()
+    gate_up_whole(1, 0, 8)
+
+    @pl.when(inner)
+    def _():
+        relay_both(DOWN, 2)
+
+    relay_both(DOWN, 3)
+    gate_up_whole(1, 8, 2 * units // 256)
+    activate(1)
+    down_second(0)
     relay_y(DOWN, 1)
-    for slot in (0, 1):
-        wait_sib(DOWN, slot)
-        down_first(slot)
-    relay_both(DOWN, 2)
-
-    @pl.when(outer)
-    def _():
-        relay_both(DOWN, 3)
-
-    gate_up(1, 0, n_cols)
-    activate(1)
-    for slot in (3, 2):
-        relay_y(DOWN, slot)
-    for slot in (0, 1):
-        down_second(slot)
-    for slot in (3, 2):
-        wait_sib(DOWN, slot)
-        down_first(slot)
-    for slot in (0, 1):
-        combine(slot)
-    for slot in (3, 2):
-        down_second(slot)
-        combine(slot)
-    for slot in (0, 1, 3, 2):
+    wait_sib(DOWN, 1)
+    down_second(1)
+    down_first(1)
+    relay_y(DOWN, 2)
+    combine(0)
+    wait_sib(DOWN, 2)
+    down_second(2)
+    down_first(2)
+    combine(1)
+    relay_y(DOWN, 3)
+    wait_sib(DOWN, 3)
+    down_second(3)
+    down_first(3)
+    combine(2)
+    combine(3)
+    for slot in range(4):
         finish(slot)
 
     for slot in range(4):
-        here, there = out_copy(slot)
-        here.wait()
-        there.wait()
-        x_copy(slot).wait_send()
+        for copy in out_copy(slot):
+            copy.wait()
+        x_copy(0, slot).wait_send()
+        x_copy(1, slot).wait_send()
         z_copy(slot).wait_send()
 
     @pl.when(sp < n_sp - 1)
@@ -657,23 +791,30 @@
             copy.wait_send()
 
     mix_copy.wait_send()
-    for kind in range(3):
-        for i in range(2):
-            token_copy(kind, i).wait_send()
+    for i in range(2):
+        token_copy(1, i).wait_send()
+        token_copy(2, i).wait_send()
+
+        @pl.when(outer)
+        def _():
+            token_copy(0, i).wait_send()
+            token_copy(3, i).wait_send()
     for what in (GATE_UP, DOWN):
-        first_sends(what, "wait_send")
+        first_sends(what, "wait_send", "own")
+        for plane in ("away", "toward", "toward_crossing"):
+            first_sends(what, "wait_send", plane)
         for slot in range(4):
             for dx in range(2):
-                p = piece(slot, dx)
+                p = piece(what, slot, dx)
                 y_copy(what, p, 2 * slot + dx).wait_send()
                 for dy in range(2):
-                    sib_copy(what, piece(slot, dx, dy)).wait_send()
+                    sib_copy(what, piece(what, slot, dx, dy)).wait_send()
         for dx in range(2):
-            far_copy(what, piece(0, dx), dx).wait_send()
+            far_copy(what, piece(what, 0, dx), dx).wait_send()
 
             @pl.when(inner)
             def _():
-                far_copy(what, piece(3, dx), 2 + dx).wait_send()
+                far_copy(what, piece(what, 1, dx), 2 + dx).wait_send()
 
 
 def fused_on_device(
@@ -702,11 +843,11 @@
             pltpu.VMEM((width, 2 * units), bf16),
             pltpu.VMEM((units, width), bf16),
             pltpu.VMEM((4 * half, width), bf16),
-            pltpu.VMEM((2 * half, 2 * units), f32),
+            pltpu.VMEM((4 * half, 2 * units), f32),
             pltpu.VMEM((4 * half, units), bf16),
-            pltpu.VMEM((2 * half, width), bf16),
+            pltpu.VMEM((2, half, width), bf16),
             pltpu.VMEM((half, width), bf16),
-            pltpu.VMEM((2 * half, width), bf16),
+            pltpu.VMEM((2, half, width), bf16),
             pltpu.VMEM((half, width), bf16),
             pltpu.VMEM((half, width), f32),
             pltpu.VMEM(queries.shape, bf16),
@@ -722,10 +863,10 @@
             pltpu.VMEM((half, width), bf16),
             dma((6,)), dma((3,)), dma((3,)), dma((2, 2, 4)), dma((2,)), dma((2, 4)), dma((2, 8)),
             dma((2, pieces)), dma((2, pieces)), dma((2, pieces)),
-            dma, dma, dma((3, 2)), dma((3, 2)), dma((4,)), dma((4,)), dma((4,)), dma((4,)),
+            dma, dma, dma((4, 2)), dma((4, 2)), dma((2, 4)), dma((2, 4)), dma((4,)), dma((4,)),
             dma((4,)), dma((4,)), dma((4,)),
         ],
-        compiler_params=pltpu.CompilerParams(has_side_effects=True, vmem_limit_bytes=63 * 2**20),
+        compiler_params=pltpu.CompilerParams(has_side_effects=True, collective_id=0, vmem_limit_bytes=63 * 2**20),
         name="layer",
     )(
         queries, key_rows, values, docs, sink_logits, residual, out_weight,

time: 198 us -> 152 us (0.77)
  Pallas kernels: 195 us -> 148 us
    pallas_call x1, Pallas kernels: 195 us -> 148 us  [fused_on_device(): pl.pallas_call(layer_kernel, out_shape=jax.ShapeDtypeStruct((rows, width)...]
where the time goes in v1:
time: 152 us; the launch traced here: 151 us
  Pallas kernels  148 us (97%)
  local copies, waits for them, and re-layouts  3.16 us (2%)
    pallas_call x1, Pallas kernels, fused_on_device(): pl.pallas_call(layer_kernel, out_shape=jax.ShapeDtypeStruct((rows, width)...  148 us
    unnamed x1, local copies, waits for them, and re-layouts  3.16 us

profile of v1, /device:TPU:17, one launch (start us, length us, event | category | flops | bytes accessed | tf_op | source)
XLA Modules:
  0.0 151.0 jit_solution(12284794795002994105)
XLA Ops:
  0.0 147.9 %layer.1 = bf16[512,2048]{1,0:T(8,128)(2,1)} custom-call(bf16[512,512]{1,0:T(8,128)(2,1)} %q_hbm.1, bf16[512,256]{1,0:T(8,128)(2,1)} %k_hbm.1, bf16[512,256]{1,0:T(8,128)(2,1)} %v_hbm.1, s32[4,1,128]{2,1,0:T(1,128)} %bitcast.3, f32[8]{0:T(128)} %sink_ref.1, bf16[512,2048]{1,0:T(8,128)(2,1)} %res_hbm.1, bf16[512,2048]{1,0:T(8,128)(2,1)} %ow_hbm.1, ...), custom_call_target="tpu_custom_call" | custom-call | tf_op jit(solution)/shard_map/layer/pallas_call | solution.py:831
  147.9 3.2 %copy.13 = bf16[512,2048]{1,0:T(8,128)(2,1)} copy(bf16[512,2048]{1,0:T(8,128)(2,1)} %layer.1) | data formatting | bytes 4194304

commit v2 on v1

--- a/solution.py
+++ b/solution.py
@@ -662,8 +662,9 @@
 
         @pl.when(inner)
         def _():
-            await_tokens(2)
-            await_tokens(3)
+            token_copy(2, 0).wait_recv()
+            token_copy(3, 0).wait_recv()
+            token_copy(0, 1).wait_recv()
 
     def send_tokens(kind, i):
         token_copy(kind, i).start()
@@ -696,6 +697,7 @@
         send_tokens(2, 1)
         relay(DOWN, 0, 1, onward=False)
         await_tokens(1)
+        forward_tokens(1, 0)
 
     @pl.when(outer)
     def _():
@@ -703,7 +705,7 @@
         for plane in ("toward_crossing", "toward"):
             first_sends(DOWN, "start", plane)
         forward_tokens(0, 3)
-        forward_tokens(1, 3)
+        token_copy(1, 1).wait_recv()
         forward_tokens(0, 0)
         relay_y(GATE_UP, 1)
         relay(GATE_UP, 3, 0)
@@ -716,7 +718,7 @@
     def _():
         relay(GATE_UP, 3, 0)
         relay_y(GATE_UP, 2)
-        for plane in ("toward_crossing", "toward"):
+        for plane in ("away", "toward_crossing", "toward"):
             first_sends(DOWN, "start", plane)
 
     @pl.when(outer)
@@ -725,11 +727,10 @@
 
     wait_sib(GATE_UP, 1)
     gate_up(0, 1)
+    for dx in range(2):
+        far_copy(DOWN, piece(DOWN, 0, dx), dx).start()
     wait_sib(GATE_UP, 2)
     gate_up(0, 2)
-    first_sends(DOWN, "start", "away")
-    for dx in range(2):
-        far_copy(DOWN, piece(DOWN, 0, dx), dx).start()
 
     @pl.when(inner)
     def _():
@@ -739,39 +740,62 @@
     relay_y(DOWN, 0)
     wait_sib(GATE_UP, 3)
     gate_up(0, 3)
+
+    @pl.when(outer)
+    def _():
+        relay_both(DOWN, 1)
+
     activate(0)
     wait_sib(DOWN, 0)
     down_first(0)
 
+    @pl.when(inner)
+    def _():
+        relay_y(DOWN, 1)
+
+    await_diagonal()
+    gate_up_whole(1, 0, 4)
+
+    @pl.when(inner)
+    def _():
+        wait_sib(DOWN, 1)
+        down_first(1)
+
     @pl.when(outer)
     def _():
-        relay_both(DOWN, 1)
         relay_both(DOWN, 2)
 
-    await_diagonal()
-    gate_up_whole(1, 0, 8)
+    gate_up_whole(1, 4, 8)
 
     @pl.when(inner)
     def _():
         relay_both(DOWN, 2)
 
-    relay_both(DOWN, 3)
     gate_up_whole(1, 8, 2 * units // 256)
     activate(1)
     down_second(0)
-    relay_y(DOWN, 1)
-    wait_sib(DOWN, 1)
+    relay_both(DOWN, 3)
+
+    @pl.when(outer)
+    def _():
+        relay_y(DOWN, 1)
+        wait_sib(DOWN, 1)
+
     down_second(1)
-    down_first(1)
     relay_y(DOWN, 2)
     combine(0)
     wait_sib(DOWN, 2)
     down_second(2)
+
+    @pl.when(outer)
+    def _():
+        down_first(1)
+
     down_first(2)
-    combine(1)
     relay_y(DOWN, 3)
     wait_sib(DOWN, 3)
     down_second(3)
+    combine(1)
     down_first(3)
     combine(2)
     combine(3)
@@ -794,11 +818,13 @@
     for i in range(2):
         token_copy(1, i).wait_send()
         token_copy(2, i).wait_send()
-
-        @pl.when(outer)
-        def _():
-            token_copy(0, i).wait_send()
-            token_copy(3, i).wait_send()
+    token_copy(0, 1).wait_send()
+
+    @pl.when(outer)
+    def _():
+        token_copy(0, 0).wait_send()
+        token_copy(3, 0).wait_send()
+
     for what in (GATE_UP, DOWN):
         first_sends(what, "wait_send", "own")
         for plane in ("away", "toward", "toward_crossing"):

time: 152 us -> 150 us (0.987)
  Pallas kernels: 148 us -> 145 us
    pallas_call x1, Pallas kernels: 148 us -> 145 us  [fused_on_device(): pl.pallas_call(layer_kernel, out_shape=jax.ShapeDtypeStruct((rows, width)...]
where the time goes in v2:
time: 150 us; the launch traced here: 149 us
  Pallas kernels  145 us (97%)
  local copies, waits for them, and re-layouts  3.16 us (2%)
    pallas_call x1, Pallas kernels, fused_on_device(): pl.pallas_call(layer_kernel, out_shape=jax.ShapeDtypeStruct((rows, width)...  145 us
    unnamed x1, local copies, waits for them, and re-layouts  3.16 us

profile of v2, /device:TPU:17, one launch (start us, length us, event | category | flops | bytes accessed | tf_op | source)
XLA Modules:
  0.0 148.7 jit_solution(6240746044236183067)
XLA Ops:
  0.0 145.5 %layer.1 = bf16[512,2048]{1,0:T(8,128)(2,1)} custom-call(bf16[512,512]{1,0:T(8,128)(2,1)} %q_hbm.1, bf16[512,256]{1,0:T(8,128)(2,1)} %k_hbm.1, bf16[512,256]{1,0:T(8,128)(2,1)} %v_hbm.1, s32[4,1,128]{2,1,0:T(1,128)} %bitcast.3, f32[8]{0:T(128)} %sink_ref.1, bf16[512,2048]{1,0:T(8,128)(2,1)} %res_hbm.1, bf16[512,2048]{1,0:T(8,128)(2,1)} %ow_hbm.1, ...), custom_call_target="tpu_custom_call" | custom-call | tf_op jit(solution)/shard_map/layer/pallas_call | solution.py:857
  145.5 3.2 %copy.13 = bf16[512,2048]{1,0:T(8,128)(2,1)} copy(bf16[512,2048]{1,0:T(8,128)(2,1)} %layer.1) | data formatting | bytes 4194304

commit v3 on v2

--- a/solution.py
+++ b/solution.py
@@ -761,16 +761,8 @@
         wait_sib(DOWN, 1)
         down_first(1)
 
-    @pl.when(outer)
-    def _():
-        relay_both(DOWN, 2)
-
     gate_up_whole(1, 4, 8)
-
-    @pl.when(inner)
-    def _():
-        relay_both(DOWN, 2)
-
+    relay_both(DOWN, 2)
     gate_up_whole(1, 8, 2 * units // 256)
     activate(1)
     down_second(0)
@@ -792,10 +784,10 @@
         down_first(1)
 
     down_first(2)
+    combine(1)
     relay_y(DOWN, 3)
     wait_sib(DOWN, 3)
     down_second(3)
-    combine(1)
     down_first(3)
     combine(2)
     combine(3)

time: 150 us -> 147 us (0.980)
    pallas_call x1, Pallas kernels: 145 us -> 144 us  [fused_on_device(): pl.pallas_call(layer_kernel, out_shape=jax.ShapeDtypeStruct((rows, width)...]
where the time goes in v3:
time: 147 us
  Pallas kernels  144 us (98%)
  local copies, waits for them, and re-layouts  3.16 us (2%)
    pallas_call x1, Pallas kernels, fused_on_device(): pl.pallas_call(layer_kernel, out_shape=jax.ShapeDtypeStruct((rows, width)...  144 us
    unnamed x1, local copies, waits for them, and re-layouts  3.16 us

profile of v3, /device:TPU:17, one launch (start us, length us, event | category | flops | bytes accessed | tf_op | source)
XLA Modules:
  0.0 147.1 jit_solution(2512239999140098681)
XLA Ops:
  0.0 144.0 %layer.1 = bf16[512,2048]{1,0:T(8,128)(2,1)} custom-call(bf16[512,512]{1,0:T(8,128)(2,1)} %q_hbm.1, bf16[512,256]{1,0:T(8,128)(2,1)} %k_hbm.1, bf16[512,256]{1,0:T(8,128)(2,1)} %v_hbm.1, s32[4,1,128]{2,1,0:T(1,128)} %bitcast.3, f32[8]{0:T(128)} %sink_ref.1, bf16[512,2048]{1,0:T(8,128)(2,1)} %res_hbm.1, bf16[512,2048]{1,0:T(8,128)(2,1)} %ow_hbm.1, ...), custom_call_target="tpu_custom_call" | custom-call | tf_op jit(solution)/shard_map/layer/pallas_call | solution.py:849
  144.0 3.2 %copy.13 = bf16[512,2048]{1,0:T(8,128)(2,1)} copy(bf16[512,2048]{1,0:T(8,128)(2,1)} %layer.1) | data formatting | bytes 4194304
